TPU v7x, 32 devices: a whole 2x2x4 slice. The times are simulated.
32 devices in a mesh: grp: 2 (over y), ra: 4 (over z), cb: 4 (over x, core).
Axes of the slice: x: 2, y: 2, z: 4, core: 2. Of those that a mesh axis runs over, the one named last changes fastest.
Arguments:
- residual: bfloat16 [512, 4096], P('grp', 'ra'), parts along dimension 0, may hold values from -6 to 6
- gain_first: bfloat16 [4096], P('ra'), may hold values from 0.099609375 to 1.8984375
- gate_first: bfloat16 [4096, 11264], P('ra', 'cb'), may hold values from -0.09375 to 0.09375
- up_first: bfloat16 [4096, 11264], P('ra', 'cb'), may hold values from -0.09375 to 0.09375
- down_first: bfloat16 [11264, 4096], P('cb', 'ra'), may hold values from -0.078125 to 0.078125
- gain_second: bfloat16 [4096], P('ra'), may hold values from 0.099609375 to 1.8984375
- gate_second: bfloat16 [4096, 11264], P('ra', 'cb'), may hold values from -0.09375 to 0.09375
- up_second: bfloat16 [4096, 11264], P('ra', 'cb'), may hold values from -0.09375 to 0.09375
- down_second: bfloat16 [11264, 4096], P('cb', 'ra'), may hold values from -0.078125 to 0.078125
Outputs:
- updated: bfloat16 [512, 4096], P('grp', 'ra'), parts along dimension 0
There are 2 independent parts, one for each index of `grp`. A program takes and returns all parts, laid end to end along the dimension named above; an argument that names none is the same for every part. Nothing has to cross between parts.
All inputs are finite; a program needn't handle non-finite values.
Results may differ from a plain program's by a relative error of at most 0.0071.
Values may be sent and summed in bfloat16 or wider, within the bound.
A program may use at most 128 MiB of HBM per device.

v0:
```python
import jax
import jax.numpy as jnp
from jax import lax
from jax.sharding import PartitionSpec as P

D = 4096
epsilon = 1e-06


def half_step(stream, gain, w_gate, w_up, w_down):
    values = stream.astype(jnp.float32)
    square_part = jnp.sum(values * values, axis=1, keepdims=True)
    normed = (values * gain.astype(jnp.float32)).astype(jnp.bfloat16)
    gate_part = jnp.dot(normed, w_gate, preferred_element_type=jnp.float32)
    up_part = jnp.dot(normed, w_up, preferred_element_type=jnp.float32)
    gate_sum, up_sum, square_sum = (
        lax.psum_scatter(gate_part, "ra", scatter_dimension=0, tiled=True),
        lax.psum_scatter(up_part, "ra", scatter_dimension=0, tiled=True),
        lax.psum_scatter(square_part, "ra", scatter_dimension=0, tiled=True),
    )
    scale = lax.rsqrt(square_sum / D + epsilon)
    hidden = (jax.nn.silu(scale * gate_sum) * (scale * up_sum)).astype(jnp.bfloat16)
    down_part = jnp.dot(
        lax.all_gather(hidden, "ra", axis=0, tiled=True), w_down, preferred_element_type=jnp.float32
    )
    branch = lax.psum(down_part, "cb")
    return (values + 0.5 * branch).astype(jnp.bfloat16)


def per_device(
    residual,
    gain_first,
    gate_first,
    up_first,
    down_first,
    gain_second,
    gate_second,
    up_second,
    down_second,
):
    middle = half_step(residual, gain_first, gate_first, up_first, down_first)
    return half_step(middle, gain_second, gate_second, up_second, down_second)


def solution(mesh):
    in_specs = (
        P("grp", "ra"),
        P("ra"),
        P("ra", "cb"),
        P("ra", "cb"),
        P("cb", "ra"),
        P("ra"),
        P("ra", "cb"),
        P("ra", "cb"),
        P("cb", "ra"),
    )
    out_specs = P("grp", "ra")
    return jax.shard_map(
        per_device, mesh=mesh, in_specs=in_specs, out_specs=out_specs, check_vma=False
    )
```

profile of v0, /device:TPU:0, one launch (start us, length us, event | category | flops | bytes accessed | tf_op | source)
XLA Modules:
  0.0 450.0 jit_solution(18293002607253876413)
XLA Ops:
  6.5 1.2 fusion
  7.8 0.8 copy.10
  8.6 0.0 reduce-scatter.13.cloned.1.call-start
  8.6 0.7 convert_element_type.31
  9.3 6.1 %fusion.10 = f32[256,2816]{1,0:T(8,128)} fusion(bf16[1024,2816]{1,0:T(8,128)(2,1)} %param.12, bf16[256,1024]{1,0:T(8,128)(2,1)} %param.9, f32[1024]{0:T(1024)S(1)} %convert_element_type.31), kind=kOutput, calls=%fused_computation.16 | convolution fusion | flops 1477181440 | bytes 9179136 | tf_op jit(solution)/shard_map/dot_general | solution.py:15
  15.4 0.0 reduce-scatter.11.cloned.1.call-start
  15.5 5.9 %fusion.12 = f32[256,2816]{1,0:T(8,128)} fusion(bf16[1024,2816]{1,0:T(8,128)(2,1)} %param.11, bf16[256,1024]{1,0:T(8,128)(2,1)S(1)} %copy-done, f32[1024]{0:T(1024)S(1)} %convert_element_type.31), kind=kOutput, calls=%fused_computation.17 | convolution fusion | flops 1477181440 | bytes 9179136 | tf_op jit(solution)/shard_map/dot_general | solution.py:14
  21.5 0.0 all-gather.3.cloned.1.call-start
  21.5 10.3 %reduce-scatter.19.cloned.1.call-done = f32[64,1]{1,0:T(8,128)} async-done(((f32[256,1]{1,0:T(8,128)}), f32[64,1]{1,0:T(8,128)}) %reduce-scatter.19.cloned.1.call-update) | async-done | bytes 272
  31.8 0.8 add_rsqrt_fusion.1
  32.5 0.1 copy.14
  32.6 56.0 %reduce-scatter.13.cloned.1.call-done = f32[64,2816]{1,0:T(8,128)} async-done(((f32[256,2816]{1,0:T(8,128)}), f32[64,2816]{1,0:T(8,128)}) %reduce-scatter.13.cloned.1.call-update) | async-done | bytes 720912 | tf_op jit(solution)/shard_map/reduce_scatter | solution.py:18
  88.6 58.4 %reduce-scatter.11.cloned.1.call-done = f32[64,2816]{1,0:T(8,128)} async-done(((f32[256,2816]{1,0:T(8,128)}), f32[64,2816]{1,0:T(8,128)}) %reduce-scatter.11.cloned.1.call-update) | async-done | bytes 720912 | tf_op jit(solution)/shard_map/reduce_scatter | solution.py:17
  147.0 2.3 multiply_convert_fusion.1
  149.4 34.6 %all-gather.3.cloned.1.call-done = bf16[256,2816]{1,0:T(8,128)(2,1)} async-done(((bf16[64,2816]{1,0:T(8,128)(2,1)}), bf16[256,2816]{1,0:T(8,128)(2,1)}) %all-gather.3.cloned.1.call-update) | async-done | bytes 1441808 | tf_op jit(solution)/shard_map/all_gather | solution.py:24
  184.1 5.7 %fusion.15 = f32[256,1024]{1,0:T(8,128)} fusion(bf16[256,2816]{1,0:T(8,128)(2,1)} %all-gather.3.cloned.1.call-done, bf16[2816,1024]{1,0:T(8,128)(2,1)} %param.13), kind=kOutput, calls=%fused_computation.20 | convolution fusion | flops 1476395008 | bytes 8257536 | tf_op jit(solution)/shard_map/dot_general | solution.py:23
  189.8 35.4 %all-reduce.3.cloned.1.call-done = f32[256,1024]{1,0:T(8,128)} async-done(((f32[256,1024]{1,0:T(8,128)}), f32[256,1024]{1,0:T(8,128)}) %all-reduce.3.cloned.1.call-update) | async-done | bytes 1048592 | tf_op jit(solution)/shard_map/psum | solution.py:26
  225.2 1.5 fusion.3
  226.7 0.8 copy.12
  227.6 5.9 %fusion.8 = f32[256,2816]{1,0:T(8,128)} fusion(bf16[1024,2816]{1,0:T(8,128)(2,1)} %param.15, bf16[256,1024]{1,0:T(8,128)(2,1)S(1)} %get-tuple-element.6, f32[1024]{0:T(1024)S(1)} %convert_element_type.36), kind=kOutput, calls=%fused_computation.15 | convolution fusion | flops 1477181440 | bytes 9179136 | tf_op jit(solution)/shard_map/dot_general | solution.py:14
  233.5 5.9 %fusion.6 = f32[256,2816]{1,0:T(8,128)} fusion(bf16[1024,2816]{1,0:T(8,128)(2,1)} %param.16, bf16[256,1024]{1,0:T(8,128)(2,1)S(1)} %get-tuple-element.6, f32[1024]{0:T(1024)S(1)} %convert_element_type.36), kind=kOutput, calls=%fused_computation.14 | convolution fusion | flops 1477181440 | bytes 9179136 | tf_op jit(solution)/shard_map/dot_general | solution.py:15
  239.6 8.1 %reduce-scatter.21.cloned.1.call-done = f32[64,1]{1,0:T(8,128)} async-done(((f32[256,1]{1,0:T(8,128)}), f32[64,1]{1,0:T(8,128)}) %reduce-scatter.21.cloned.1.call-update) | async-done | bytes 272
  247.6 0.8 add_rsqrt_fusion
  248.4 0.1 copy.15
  248.5 56.0 %reduce-scatter.15.cloned.1.call-done = f32[64,2816]{1,0:T(8,128)} async-done(((f32[256,2816]{1,0:T(8,128)}), f32[64,2816]{1,0:T(8,128)}) %reduce-scatter.15.cloned.1.call-update) | async-done | bytes 720912 | tf_op jit(solution)/shard_map/reduce_scatter | solution.py:17
  304.4 58.4 %reduce-scatter.17.cloned.1.call-done = f32[64,2816]{1,0:T(8,128)} async-done(((f32[256,2816]{1,0:T(8,128)}), f32[64,2816]{1,0:T(8,128)}) %reduce-scatter.17.cloned.1.call-update) | async-done | bytes 720912 | tf_op jit(solution)/shard_map/reduce_scatter | solution.py:18
  362.9 2.3 multiply_convert_fusion
  365.2 0.0 all-reduce.5.cloned.1.call-start
  365.3 34.6 %all-gather.5.cloned.1.call-done = bf16[256,2816]{1,0:T(8,128)(2,1)} async-done(((bf16[64,2816]{1,0:T(8,128)(2,1)}), bf16[256,2816]{1,0:T(8,128)(2,1)}) %all-gather.5.cloned.1.call-update) | async-done | bytes 1441808 | tf_op jit(solution)/shard_map/all_gather | solution.py:24
  399.9 5.7 %fusion.16 = f32[256,1024]{1,0:T(8,128)} fusion(bf16[256,2816]{1,0:T(8,128)(2,1)} %all-gather.5.cloned.1.call-done, bf16[2816,1024]{1,0:T(8,128)(2,1)} %param.17), kind=kOutput, calls=%fused_computation.21 | convolution fusion | flops 1476395008 | bytes 8257536 | tf_op jit(solution)/shard_map/dot_general | solution.py:23
  405.6 35.4 %all-reduce.5.cloned.1.call-done = f32[256,1024]{1,0:T(8,128)} async-done(((f32[256,1024]{1,0:T(8,128)}), f32[256,1024]{1,0:T(8,128)}) %all-reduce.5.cloned.1.call-update) | async-done | bytes 1048592 | tf_op jit(solution)/shard_map/psum | solution.py:26
  441.0 2.2 fusion.5
  (21 shorter events, 0.4 us)
Async XLA Ops:
  6.5 25.2 %reduce-scatter.19.cloned.1.call-start = ((), (), s32[]{:S(2)}) async-start(), calls=%async_computation.14 | async-start | bytes 163840
  8.6 80.0 %reduce-scatter.13.cloned.1.call-start = ((), (), s32[]{:S(2)}) async-start(), calls=%async_computation.7 | async-start | bytes 3604480 | tf_op jit(solution)/shard_map/reduce_scatter | solution.py:18
  9.3 6.2 %copy-start = (bf16[256,1024]{1,0:T(8,128)(2,1)S(1)}, bf16[256,1024]{1,0:T(8,128)(2,1)}, u32[]{:S(2)}) copy-start(bf16[256,1024]{1,0:T(8,128)(2,1)} %param.9) | copy-start | bytes 1572868
  15.4 131.6 %reduce-scatter.11.cloned.1.call-start = ((), (), s32[]{:S(2)}) async-start(), calls=%async_computation.6 | async-start | bytes 3604480 | tf_op jit(solution)/shard_map/reduce_scatter | solution.py:17
  21.5 162.6 %all-gather.3.cloned.1.call-start = ((), (), s32[]{:S(2)}) async-start(), calls=%async_computation.8 | async-start | bytes 1802240 | tf_op jit(solution)/shard_map/all_gather | solution.py:24
  149.4 40.4 %copy-start.1 = (bf16[1024]{0:T(1024)(128)(2,1)S(1)}, bf16[1024]{0:T(1024)(128)(2,1)}, u32[]{:S(2)}) copy-start(bf16[1024]{0:T(1024)(128)(2,1)} %param.14) | copy-start | bytes 6148
  149.4 75.8 %all-reduce.3.cloned.1.call-start = ((), (), s32[]{:S(2)}) async-start(), calls=%async_computation.9 | async-start | bytes 2097152 | tf_op jit(solution)/shard_map/psum | solution.py:26
  189.8 57.9 %reduce-scatter.21.cloned.1.call-start = ((), (), s32[]{:S(2)}) async-start(), calls=%async_computation.15 | async-start | bytes 163840
  227.5 76.9 %reduce-scatter.15.cloned.1.call-start = ((), (), s32[]{:S(2)}) async-start(), calls=%async_computation.10 | async-start | bytes 3604480 | tf_op jit(solution)/shard_map/reduce_scatter | solution.py:17
  233.5 129.4 %reduce-scatter.17.cloned.1.call-start = ((), (), s32[]{:S(2)}) async-start(), calls=%async_computation.11 | async-start | bytes 3604480 | tf_op jit(solution)/shard_map/reduce_scatter | solution.py:18
  239.5 160.4 %all-gather.5.cloned.1.call-start = ((), (), s32[]{:S(2)}) async-start(), calls=%async_computation.12 | async-start | bytes 1802240 | tf_op jit(solution)/shard_map/all_gather | solution.py:24
  365.2 75.8 %all-reduce.5.cloned.1.call-start = ((), (), s32[]{:S(2)}) async-start(), calls=%async_computation.13 | async-start | bytes 2097152 | tf_op jit(solution)/shard_map/psum | solution.py:26
Sparse Core Ops, SparseCore 0:
  9.6 22.1 reduce-scatter.18
  34.1 54.4 reduce-scatter.12
  90.9 56.0 reduce-scatter.10
  149.5 34.5 all-gather.2
  189.9 35.2 all-reduce.2
  227.6 19.9 reduce-scatter.20
  249.9 54.4 reduce-scatter.14
  306.7 56.0 reduce-scatter.16
  365.3 34.5 all-gather.4
  405.7 35.2 all-reduce.4
where the time goes:
time: 451 us; the launch traced here: 450 us
  waiting for transfers between devices  387 us (86%)
  matrix products  35.2 us (8%)
  between operations  13.6 us (3%)
  other arithmetic  11.8 us (3%)
    reduce_scatter x2, waiting for transfers between devices, half_step(): lax.psum_scatter(up_part, 'ra', scatter_dimension=0, tiled=True)  114 us
    reduce_scatter x2, waiting for transfers between devices, half_step(): lax.psum_scatter(gate_part, 'ra', scatter_dimension=0, tiled=True)  114 us
    psum x2, waiting for transfers between devices, half_step(): branch = lax.psum(down_part, 'cb')  70.8 us
    all_gather x2, waiting for transfers between devices, half_step(): lax.all_gather(hidden, 'ra', axis=0, tiled=True)  69.2 us
    unnamed x12, waiting for transfers between devices  18.5 us
    dot_general x2, matrix products, half_step(): up_part = jnp.dot(normed, w_up, preferred_element_type=jnp.float32)  12 us
    dot_general x2, matrix products, half_step(): gate_part = jnp.dot(normed, w_gate, preferred_element_type=jnp.float32)  11.8 us
    dot_general x2, matrix products, half_step(): jnp.dot(lax.all_gather(hidden, 'ra', axis=0, tiled=True), w_down, preferr...  11.4 us
  transfers between devices with their start and end apart: 10, of which 10 were waited for; matrix products, arithmetic and copies ran while one was open for 6% of the time, Pallas kernels for 0%

commit v1 on v0

--- a/solution.py
+++ b/solution.py
@@ -23,7 +23,8 @@
     down_part = jnp.dot(
         lax.all_gather(hidden, "ra", axis=0, tiled=True), w_down, preferred_element_type=jnp.float32
     )
-    branch = lax.psum(down_part, "cb")
+    x_new = lax.all_gather(down_part, "cb")
+    branch = jnp.sum(x_new, axis=0)
     return (values + 0.5 * branch).astype(jnp.bfloat16)
 
 

time: 451 us -> 450 us (level)
    psum x2 -> x0, waiting for transfers between devices: 70.8 us -> none  [half_step(): branch = lax.psum(down_part, 'cb')]
    all_gather x0 -> x2, waiting for transfers between devices: none -> 67.1 us  [half_step(): x_new = lax.all_gather(down_part, 'cb')]
    reduce_sum x0 -> x2, other arithmetic: none -> 5.44 us  [half_step(): branch = jnp.sum(x_new, axis=0)]
where the time goes in v1:
time: 450 us; the launch traced here: 449 us
  waiting for transfers between devices  383 us (85%)
  matrix products  35.3 us (8%)
  other arithmetic  14.8 us (3%)
  between operations  13.6 us (3%)
    reduce_scatter x2, waiting for transfers between devices, half_step(): lax.psum_scatter(up_part, 'ra', scatter_dimension=0, tiled=True)  114 us
    reduce_scatter x2, waiting for transfers between devices, half_step(): lax.psum_scatter(gate_part, 'ra', scatter_dimension=0, tiled=True)  114 us
    all_gather x2, waiting for transfers between devices, half_step(): lax.all_gather(hidden, 'ra', axis=0, tiled=True)  69.2 us
    all_gather x2, waiting for transfers between devices, half_step(): x_new = lax.all_gather(down_part, 'cb')  67.1 us
    unnamed x12, waiting for transfers between devices  18 us
    dot_general x2, matrix products, half_step(): up_part = jnp.dot(normed, w_up, preferred_element_type=jnp.float32)  12 us
    dot_general x2, matrix products, half_step(): gate_part = jnp.dot(normed, w_gate, preferred_element_type=jnp.float32)  11.8 us
    dot_general x2, matrix products, half_step(): jnp.dot(lax.all_gather(hidden, 'ra', axis=0, tiled=True), w_down, preferr...  11.4 us
  transfers between devices with their start and end apart: 10, of which 10 were waited for; matrix products, arithmetic and copies ran while one was open for 6% of the time, Pallas kernels for 0%

profile of v1, /device:TPU:0, one launch (start us, length us, event | category | flops | bytes accessed | tf_op | source)
XLA Modules:
  0.0 448.9 jit_solution(3726252501181231483)
XLA Ops:
  6.5 1.2 fusion
  7.8 0.8 copy.10
  8.6 0.0 reduce-scatter.13.cloned.1.call-start
  8.6 0.7 convert_element_type.31
  9.3 6.1 %fusion.10 = f32[256,2816]{1,0:T(8,128)} fusion(bf16[1024,2816]{1,0:T(8,128)(2,1)} %param.12, bf16[256,1024]{1,0:T(8,128)(2,1)} %param.9, f32[1024]{0:T(1024)S(1)} %convert_element_type.31), kind=kOutput, calls=%fused_computation.16 | convolution fusion | flops 1477181440 | bytes 9179136 | tf_op jit(solution)/shard_map/dot_general | solution.py:15
  15.4 0.0 reduce-scatter.11.cloned.1.call-start
  15.5 5.9 %fusion.12 = f32[256,2816]{1,0:T(8,128)} fusion(bf16[1024,2816]{1,0:T(8,128)(2,1)} %param.11, bf16[256,1024]{1,0:T(8,128)(2,1)S(1)} %copy-done, f32[1024]{0:T(1024)S(1)} %convert_element_type.31), kind=kOutput, calls=%fused_computation.17 | convolution fusion | flops 1477181440 | bytes 9179136 | tf_op jit(solution)/shard_map/dot_general | solution.py:14
  21.5 10.3 %reduce-scatter.19.cloned.1.call-done = f32[64,1]{1,0:T(8,128)} async-done(((f32[256,1]{1,0:T(8,128)}), f32[64,1]{1,0:T(8,128)}) %reduce-scatter.19.cloned.1.call-update) | async-done | bytes 272
  31.8 0.8 add_rsqrt_fusion.1
  32.5 0.1 copy.14
  32.6 56.0 %reduce-scatter.13.cloned.1.call-done = f32[64,2816]{1,0:T(8,128)} async-done(((f32[256,2816]{1,0:T(8,128)}), f32[64,2816]{1,0:T(8,128)}) %reduce-scatter.13.cloned.1.call-update) | async-done | bytes 720912 | tf_op jit(solution)/shard_map/reduce_scatter | solution.py:18
  88.6 58.4 %reduce-scatter.11.cloned.1.call-done = f32[64,2816]{1,0:T(8,128)} async-done(((f32[256,2816]{1,0:T(8,128)}), f32[64,2816]{1,0:T(8,128)}) %reduce-scatter.11.cloned.1.call-update) | async-done | bytes 720912 | tf_op jit(solution)/shard_map/reduce_scatter | solution.py:17
  147.0 2.3 multiply_convert_fusion.1
  149.4 34.6 %all-gather.7.cloned.1.call-done = bf16[256,2816]{1,0:T(8,128)(2,1)} async-done(((bf16[64,2816]{1,0:T(8,128)(2,1)}), bf16[256,2816]{1,0:T(8,128)(2,1)}) %all-gather.7.cloned.1.call-update) | async-done | bytes 1441808 | tf_op jit(solution)/shard_map/all_gather | solution.py:24
  184.1 5.7 %fusion.15 = f32[256,1024]{1,0:T(8,128)} fusion(bf16[256,2816]{1,0:T(8,128)(2,1)} %all-gather.7.cloned.1.call-done, bf16[2816,1024]{1,0:T(8,128)(2,1)} %param.13), kind=kOutput, calls=%fused_computation.20 | convolution fusion | flops 1476395008 | bytes 8257536 | tf_op jit(solution)/shard_map/dot_general | solution.py:23
  189.9 33.5 %all-gather.11.cloned.1.call-done = f32[1024,1024]{1,0:T(8,128)} async-done(((f32[256,1024]{1,0:T(8,128)}), f32[1024,1024]{1,0:T(8,128)}) %all-gather.11.cloned.1.call-update) | async-done | bytes 4194320 | tf_op jit(solution)/shard_map/all_gather | solution.py:26
  223.4 2.7 reduce_sum.37
  226.1 0.3 fusion.3
  226.4 0.8 copy.12
  227.3 5.9 %fusion.8 = f32[256,2816]{1,0:T(8,128)} fusion(bf16[1024,2816]{1,0:T(8,128)(2,1)} %param.15, bf16[256,1024]{1,0:T(8,128)(2,1)S(1)} %get-tuple-element.6, f32[1024]{0:T(1024)S(1)} %convert_element_type.36), kind=kOutput, calls=%fused_computation.15 | convolution fusion | flops 1477181440 | bytes 9179136 | tf_op jit(solution)/shard_map/dot_general | solution.py:14
  233.2 5.9 %fusion.6 = f32[256,2816]{1,0:T(8,128)} fusion(bf16[1024,2816]{1,0:T(8,128)(2,1)} %param.16, bf16[256,1024]{1,0:T(8,128)(2,1)S(1)} %get-tuple-element.6, f32[1024]{0:T(1024)S(1)} %convert_element_type.36), kind=kOutput, calls=%fused_computation.14 | convolution fusion | flops 1477181440 | bytes 9179136 | tf_op jit(solution)/shard_map/dot_general | solution.py:15
  239.2 7.6 %reduce-scatter.21.cloned.1.call-done = f32[64,1]{1,0:T(8,128)} async-done(((f32[256,1]{1,0:T(8,128)}), f32[64,1]{1,0:T(8,128)}) %reduce-scatter.21.cloned.1.call-update) | async-done | bytes 272
  246.8 0.8 add_rsqrt_fusion
  247.6 0.1 copy.15
  247.7 56.0 %reduce-scatter.15.cloned.1.call-done = f32[64,2816]{1,0:T(8,128)} async-done(((f32[256,2816]{1,0:T(8,128)}), f32[64,2816]{1,0:T(8,128)}) %reduce-scatter.15.cloned.1.call-update) | async-done | bytes 720912 | tf_op jit(solution)/shard_map/reduce_scatter | solution.py:17
  303.7 58.4 %reduce-scatter.17.cloned.1.call-done = f32[64,2816]{1,0:T(8,128)} async-done(((f32[256,2816]{1,0:T(8,128)}), f32[64,2816]{1,0:T(8,128)}) %reduce-scatter.17.cloned.1.call-update) | async-done | bytes 720912 | tf_op jit(solution)/shard_map/reduce_scatter | solution.py:18
  362.1 2.3 multiply_convert_fusion
  364.5 34.6 %all-gather.9.cloned.1.call-done = bf16[256,2816]{1,0:T(8,128)(2,1)} async-done(((bf16[64,2816]{1,0:T(8,128)(2,1)}), bf16[256,2816]{1,0:T(8,128)(2,1)}) %all-gather.9.cloned.1.call-update) | async-done | bytes 1441808 | tf_op jit(solution)/shard_map/all_gather | solution.py:24
  399.1 5.7 %fusion.16 = f32[256,1024]{1,0:T(8,128)} fusion(bf16[256,2816]{1,0:T(8,128)(2,1)} %all-gather.9.cloned.1.call-done, bf16[2816,1024]{1,0:T(8,128)(2,1)} %param.17), kind=kOutput, calls=%fused_computation.21 | convolution fusion | flops 1476395008 | bytes 8257536 | tf_op jit(solution)/shard_map/dot_general | solution.py:23
  404.8 33.6 %all-gather.13.cloned.1.call-done = f32[1024,1024]{1,0:T(8,128)} async-done(((f32[256,1024]{1,0:T(8,128)}), f32[1024,1024]{1,0:T(8,128)}) %all-gather.13.cloned.1.call-update) | async-done | bytes 4194320 | tf_op jit(solution)/shard_map/all_gather | solution.py:26
  438.4 2.7 reduce_sum.39
  441.2 1.0 fusion.5
  (23 shorter events, 0.5 us)
Async XLA Ops:
  6.5 25.2 %reduce-scatter.19.cloned.1.call-start = ((), (), s32[]{:S(2)}) async-start(), calls=%async_computation.14 | async-start | bytes 163840
  8.6 80.0 %reduce-scatter.13.cloned.1.call-start = ((), (), s32[]{:S(2)}) async-start(), calls=%async_computation.7 | async-start | bytes 3604480 | tf_op jit(solution)/shard_map/reduce_scatter | solution.py:18
  9.3 6.2 %copy-start = (bf16[256,1024]{1,0:T(8,128)(2,1)S(1)}, bf16[256,1024]{1,0:T(8,128)(2,1)}, u32[]{:S(2)}) copy-start(bf16[256,1024]{1,0:T(8,128)(2,1)} %param.9) | copy-start | bytes 1572868
  15.4 131.6 %reduce-scatter.11.cloned.1.call-start = ((), (), s32[]{:S(2)}) async-start(), calls=%async_computation.6 | async-start | bytes 3604480 | tf_op jit(solution)/shard_map/reduce_scatter | solution.py:17
  21.5 162.6 %all-gather.7.cloned.1.call-start = ((), (), s32[]{:S(2)}) async-start(), calls=%async_computation.8 | async-start | bytes 1802240 | tf_op jit(solution)/shard_map/all_gather | solution.py:24
  149.4 40.5 %copy-start.1 = (bf16[1024]{0:T(1024)(128)(2,1)S(1)}, bf16[1024]{0:T(1024)(128)(2,1)}, u32[]{:S(2)}) copy-start(bf16[1024]{0:T(1024)(128)(2,1)} %param.14) | copy-start | bytes 6148
  149.4 74.0 %all-gather.11.cloned.1.call-start = ((), (), s32[]{:S(2)}) async-start(), calls=%async_computation.12 | async-start | bytes 5242880 | tf_op jit(solution)/shard_map/all_gather | solution.py:26
  189.8 57.0 %reduce-scatter.21.cloned.1.call-start = ((), (), s32[]{:S(2)}) async-start(), calls=%async_computation.15 | async-start | bytes 163840
  227.2 76.4 %reduce-scatter.15.cloned.1.call-start = ((), (), s32[]{:S(2)}) async-start(), calls=%async_computation.9 | async-start | bytes 3604480 | tf_op jit(solution)/shard_map/reduce_scatter | solution.py:17
  233.2 128.9 %reduce-scatter.17.cloned.1.call-start = ((), (), s32[]{:S(2)}) async-start(), calls=%async_computation.10 | async-start | bytes 3604480 | tf_op jit(solution)/shard_map/reduce_scatter | solution.py:18
  239.2 159.9 %all-gather.9.cloned.1.call-start = ((), (), s32[]{:S(2)}) async-start(), calls=%async_computation.11 | async-start | bytes 1802240 | tf_op jit(solution)/shard_map/all_gather | solution.py:24
  364.4 74.0 %all-gather.13.cloned.1.call-start = ((), (), s32[]{:S(2)}) async-start(), calls=%async_computation.13 | async-start | bytes 5242880 | tf_op jit(solution)/shard_map/all_gather | solution.py:26
Sparse Core Ops, SparseCore 0:
  9.6 22.1 reduce-scatter.18
  34.1 54.4 reduce-scatter.12
  90.9 56.0 reduce-scatter.10
  149.5 34.5 all-gather.6
  189.9 33.4 all-gather.10
  227.3 19.4 reduce-scatter.20
  249.1 54.4 reduce-scatter.14
  306.0 56.0 reduce-scatter.16
  364.5 34.5 all-gather.8
  405.0 33.4 all-gather.12
